TPU v7x, 32 devices: a whole 2x2x4 slice. The times are simulated.
32 devices in a mesh: sp: 8 (over z, y), tp: 4 (over x, core).
Axes of the slice: x: 2, y: 2, z: 4, core: 2. Of those that a mesh axis runs over, the one named last changes fastest.
Arguments:
- query_rows: bfloat16 [2560, 1024], P('sp', 'tp'), may hold values from -6 to 6
- key_rows: bfloat16 [2560, 1024], P('sp', 'tp'), may hold values from -6 to 6
- value_rows: bfloat16 [2560, 1024], P('sp', 'tp'), may hold values from -6 to 6
- key_shift: bfloat16 [2560, 16], P('sp', 'tp'), may hold values from -10 to 6
- documents: int32 [2560], P('sp'), may hold values from 0 to 3, never falling along the last dimension, each value on 1 to 1280 neighbouring positions
- out_weight: bfloat16 [1024, 2048], P('tp'), may hold values from -0.1875 to 0.1875
- stream: bfloat16 [2560, 2048], P('sp', 'tp'), may hold values from -8 to 8
- norm_gain: float32 [2048], replicated, may hold values from 0.1 to 1.9
- expert_ids: int32 [2560, 2], P('sp'), may hold values from 0 to 7, all different within a row; in each aligned block of 320 rows (0 to 319, 320 to 639, ...) at most 107 rows name the same one
- expert_weights: float32 [2560, 2], P('sp'), may hold values from 0.25 to 1
- gate_weight: bfloat16 [8, 2048, 3584], P('sp', None, 'tp'), may hold values from -0.125 to 0.125
- up_weight: bfloat16 [8, 2048, 3584], P('sp', None, 'tp'), may hold values from -0.125 to 0.125
- down_weight: bfloat16 [8, 3584, 2048], P('sp', 'tp'), may hold values from -0.09375 to 0.09375
Outputs:
- layer_out: bfloat16 [2560, 2048], P('sp', 'tp')
Inputs may be any that keep to these rules, and one draw needn't show every extreme that they name: `expert_ids`: in each aligned block of 320 rows no expert is named by more than 107 rows, a bound that some block reaches; the entries of a row differ. `documents`: document numbers never fall along the positions; each document has 1 to 1280 positions, and one has exactly 1280.
All inputs are finite; a program needn't handle non-finite values.
Results may differ from a plain program's by a relative error of at most 0.013.
Values may be sent and summed in bfloat16 or wider, within the bound.
A program may use at most 128 MiB of HBM per device.

v0:
```python
import functools

import jax
import jax.numpy as jnp
from jax import lax
from jax.experimental import pallas as pl
from jax.experimental.pallas import tpu as pltpu
from jax.sharding import PartitionSpec as P

D = 2048
HEAD = 64
REACH = 4
LANES = 128
LOG2E = 1.4426950408889634

NORM_EPS = 1e-06
MESH = pl.DeviceIdType.MESH


def attention_kernel(
    count, q_ref, qdoc_ref, kv_ref, aux_ref, out_ref,
    kv_buf, aux_buf, acc, total, kv_send, kv_recv, aux_send, aux_recv,
):
    me = lax.axis_index("sp")
    odd = lax.rem(me, 2)
    even = 1 - odd
    partner = me + 1 - 2 * odd
    pairs, rows, _ = kv_ref.shape

    barrier = pltpu.get_barrier_semaphore()
    pl.semaphore_signal(barrier, inc=1, device_id={"sp": partner}, device_id_type=MESH)

    @pl.when(me + 2 < count)
    def _():
        pl.semaphore_signal(barrier, inc=1, device_id={"sp": me + 2}, device_id_type=MESH)

    @pl.when(me >= 2)
    def _():
        pl.semaphore_signal(barrier, inc=1, device_id={"sp": me - 2}, device_id_type=MESH)

    peers = 1 + jnp.where(me + 2 < count, 1, 0) + jnp.where(me >= 2, 1, 0)
    pl.semaphore_wait(barrier, peers)

    def own(item):
        return kv_ref.at[item] if item < pairs else aux_ref

    def slot(item, distance):
        return kv_buf.at[distance - 1, item] if item < pairs else aux_buf.at[distance - 1]

    def remote(item, source, distance, kind, target):
        if item < pairs:
            send, recv = kv_send.at[kind, item], kv_recv.at[distance - 1, item]
        else:
            send, recv = aux_send.at[kind], aux_recv.at[distance - 1]
        return pltpu.make_async_remote_copy(
            src_ref=source, dst_ref=slot(item, distance), send_sem=send, recv_sem=recv,
            device_id={"sp": target}, device_id_type=MESH,
        )

    has_next = me + 2 < count
    copies = {
        "chain": (has_next, lambda i: remote(i, own(i), 2, 0, me + 2)),
        "chain2": (has_next & (me >= 2), lambda i: remote(i, slot(i, 2), 4, 1, me + 2)),
        "even1": (even == 1, lambda i: remote(i, own(i), 1, 2, partner)),
        "even3": ((even == 1) & (me >= 2), lambda i: remote(i, slot(i, 2), 3, 3, partner)),
        "odd1": ((odd == 1) & (me >= 2), lambda i: remote(i, slot(i, 2), 1, 2, partner)),
        "odd3": ((odd == 1) & (me >= 4), lambda i: remote(i, slot(i, 4), 3, 3, partner)),
    }

    def start(name, items):
        condition, make = copies[name]

        @pl.when(condition)
        def _():
            for item in items:
                make(item).start()

    def arrive(distance, items):
        @pl.when(me >= distance)
        def _():
            for item in items:
                remote(item, slot(item, distance), distance, 0, partner).wait_recv()

    lane = lax.broadcasted_iota(jnp.int32, (rows, LANES), 1)
    row_of = lax.broadcasted_iota(jnp.int32, (rows, rows), 0)
    col_of = lax.broadcasted_iota(jnp.int32, (rows, rows), 1)
    later = jnp.where(row_of >= col_of, 1.0, 0.0).astype(jnp.bfloat16)
    qdoc = qdoc_ref[...]
    per_pair = LANES // HEAD

    def block(head, pair, half, distance, key_value, aux, aux_row):
        in_head = (lane >= half * HEAD) & (lane < (half + 1) * HEAD)
        cols = pl.ds(pair * LANES, LANES)
        query = q_ref[:, cols]
        query = jnp.where(in_head, query, jnp.zeros_like(query))
        scores = lax.dot_general(
            query, key_value[:, :LANES], (((1,), (1,)), ((), ())),
            preferred_element_type=jnp.float32,
        )
        scores = (scores * (HEAD ** -0.5) + aux_row(head)) * LOG2E
        admitted = qdoc == aux_row(aux.shape[0] - 1)
        if distance == 0:
            admitted = admitted & (col_of < row_of)
        rest = jnp.minimum(-scores, 0.0) - jnp.log2(1.0 + jnp.exp2(-jnp.abs(scores)))
        rest = jnp.where(admitted, rest, 0.0)
        high = rest.astype(jnp.bfloat16)
        low = (rest - high.astype(jnp.float32)).astype(jnp.bfloat16)
        suffix = jnp.dot(high, later, preferred_element_type=jnp.float32) + jnp.dot(
            low, later, preferred_element_type=jnp.float32
        )
        before = jnp.zeros((rows, 1), jnp.float32) if distance == 0 else total[head]
        weight = jnp.where(admitted, jnp.exp2(scores + suffix + before), 0.0).astype(jnp.bfloat16)
        product = jnp.dot(weight, key_value[:, LANES:], preferred_element_type=jnp.float32)
        product = jnp.where(in_head, product, 0.0)
        if distance == 0 and half == 0:
            acc[pair] = product
        else:
            acc[pair] += product
        total[head] = before + suffix[:, :1]

    def own_pair(pair):
        for half in range(per_pair):
            block(
                pair * per_pair + half, pair, half, 0, kv_ref[pair], aux_ref,
                lambda r: aux_ref[pl.ds(r, 1), :],
            )

    def far_pair(pair, distance):
        @pl.when(me >= distance)
        def _():
            for half in range(per_pair):
                block(
                    pair * per_pair + half, pair, half, distance,
                    kv_buf[distance - 1, pair], aux_buf.at[distance - 1],
                    lambda r: aux_buf[distance - 1, pl.ds(r, 1), :],
                )

    everything = (pairs,) + tuple(range(pairs))
    start("chain", everything)
    start("even1", everything)
    first, rest_items = (pairs, 0), tuple(range(1, pairs))
    own_pair(0)
    arrive(2, first)
    for name in ("chain2", "even3", "odd1"):
        start(name, first)
    for pair in range(1, pairs):
        own_pair(pair)
    arrive(2, rest_items)
    for name in ("chain2", "even3", "odd1"):
        start(name, rest_items)
    arrive(1, first)
    far_pair(0, 1)
    far_pair(0, 2)
    arrive(4, first)
    start("odd3", first)
    arrive(1, rest_items)
    for pair in range(1, pairs):
        far_pair(pair, 1)
        far_pair(pair, 2)
    arrive(4, rest_items)
    start("odd3", rest_items)
    arrive(3, first)
    far_pair(0, 3)
    far_pair(0, 4)
    arrive(3, rest_items)
    for pair in range(1, pairs):
        far_pair(pair, 3)
        far_pair(pair, 4)
    for pair in range(pairs):
        out_ref[:, pair * LANES:(pair + 1) * LANES] = acc[pair].astype(out_ref.dtype)
    for condition, make in copies.values():
        @pl.when(condition)
        def _(make=make):
            for item in everything:
                make(item).wait_send()


def attend(query_rows, key_rows, value_rows, key_shift, documents):
    count = lax.axis_size("sp")
    rows, width = query_rows.shape
    pairs = width // LANES
    key_value = jnp.stack([
        jnp.concatenate(
            [part[:, p * LANES:(p + 1) * LANES] for part in (key_rows, value_rows)], axis=1
        )
        for p in range(pairs)
    ])
    heads = key_shift.shape[1]
    docs = documents.astype(jnp.float32)
    aux = jnp.concatenate([
        jnp.transpose(key_shift).astype(jnp.float32),
        jnp.broadcast_to(docs[None, :], (8 - heads % 8, rows)),
    ])
    vmem = pl.BlockSpec(memory_space=pltpu.VMEM)
    return pl.pallas_call(
        functools.partial(attention_kernel, count),
        out_shape=jax.ShapeDtypeStruct((rows, width), jnp.bfloat16),
        in_specs=[vmem] * 4,
        out_specs=vmem,
        scratch_shapes=[
            pltpu.VMEM((REACH, pairs, rows, 2 * LANES), jnp.bfloat16),
            pltpu.VMEM((REACH,) + aux.shape, jnp.float32),
            pltpu.VMEM((pairs, rows, LANES), jnp.float32),
            pltpu.VMEM((heads, rows, 1), jnp.float32),
            pltpu.SemaphoreType.DMA((4, pairs)),
            pltpu.SemaphoreType.DMA((REACH, pairs)),
            pltpu.SemaphoreType.DMA((4,)),
            pltpu.SemaphoreType.DMA((REACH,)),
        ],
        compiler_params=pltpu.CompilerParams(collective_id=0, has_side_effects=True),
        name="attention",
    )(query_rows, docs[:, None], key_value, aux)


def shards(
    query_rows,
    key_rows,
    value_rows,
    key_shift,
    documents,
    out_weight,
    stream,
    norm_gain,
    expert_ids,
    expert_weights,
    gate_weight,
    up_weight,
    down_weight,
):
    portion_rows = query_rows.shape[0]
    attended = attend(query_rows, key_rows, value_rows, key_shift, documents)
    partial_value = jnp.dot(attended, out_weight, preferred_element_type=jnp.float32)
    projected = lax.psum_scatter(
        partial_value.astype(jnp.bfloat16), "tp", scatter_dimension=1, tiled=True
    ).astype(jnp.float32)
    middle = (stream.astype(jnp.float32) + projected).astype(jnp.bfloat16)
    middle_wide = middle.astype(jnp.float32)
    sending = middle
    top_count = expert_ids.shape[1]
    experts = lax.axis_size("sp") * gate_weight.shape[0]
    capacity = (4 * portion_rows * top_count + 3 * experts - 1) // (3 * experts)
    flat_ids = expert_ids.reshape(portion_rows * top_count)
    onehot = (flat_ids[:, None] == jnp.arange(experts, dtype=jnp.int32)[None, :]).astype(jnp.int32)
    slot_index = jnp.sum((jnp.cumsum(onehot, axis=0) - 1) * onehot, axis=1)
    target = flat_ids * capacity + slot_index
    buffer = jnp.zeros((experts * capacity, sending.shape[1]), jnp.bfloat16)
    buffer = buffer.at[target].set(jnp.repeat(sending, top_count, axis=0))
    buffer = buffer.reshape(experts, capacity, sending.shape[1])
    arrived = lax.all_to_all(buffer, "sp", split_axis=0, concat_axis=0, tiled=True)
    arrived = lax.all_gather(arrived, "tp", axis=2, tiled=True)
    sources, item_count, feat_count = arrived.shape
    row_block = arrived.reshape(sources * item_count, feat_count).astype(jnp.float32)
    square_mean = jnp.sum(row_block * row_block, axis=1, keepdims=True) / D
    row_block = (row_block * lax.rsqrt(square_mean + NORM_EPS) * norm_gain[None, :]).astype(
        jnp.bfloat16
    )
    gate_value = jnp.dot(row_block, gate_weight[0], preferred_element_type=jnp.float32)
    up_value = jnp.dot(row_block, up_weight[0], preferred_element_type=jnp.float32)
    hidden = (jax.nn.silu(gate_value) * up_value).astype(jnp.bfloat16)
    partial_out = jnp.dot(hidden, down_weight[0], preferred_element_type=jnp.float32)
    summed = lax.psum_scatter(
        partial_out.astype(jnp.bfloat16), "tp", scatter_dimension=1, tiled=True
    ).astype(jnp.float32)
    result = summed.astype(jnp.bfloat16).reshape(sources, item_count, summed.shape[1])
    returned_rows = lax.all_to_all(result, "sp", split_axis=0, concat_axis=0, tiled=True)
    picked = returned_rows.reshape(experts * capacity, returned_rows.shape[2])[target].astype(
        jnp.float32
    )
    mixed = jnp.sum(
        picked.reshape(portion_rows, top_count, picked.shape[1]) * expert_weights[:, :, None],
        axis=1,
    )
    return (middle_wide + mixed).astype(jnp.bfloat16)


def solution(mesh):
    in_specs = (
        P("sp", "tp"),
        P("sp", "tp"),
        P("sp", "tp"),
        P("sp", "tp"),
        P("sp"),
        P("tp", None),
        P("sp", "tp"),
        P(),
        P("sp", None),
        P("sp", None),
        P("sp", None, "tp"),
        P("sp", None, "tp"),
        P("sp", "tp", None),
    )
    out_specs = P("sp", "tp")
    return jax.shard_map(shards, mesh=mesh, in_specs=in_specs, out_specs=out_specs, check_vma=False)
```

profile of v0, /device:TPU:0, one launch (start us, length us, event | category | flops | bytes accessed | tf_op | source)
XLA Modules:
  0.0 252.8 jit_solution(5310341355671268859)
XLA Ops:
  6.5 0.0 copy-start
  6.5 0.0 reduce-scatter.3.cloned.1.call-start
  6.5 1.0 fusion.19
  7.6 0.9 fusion.20
  8.5 0.7 convert_element_type.61
  9.2 0.8 broadcast_in_dim.12.qdoc_ref
  10.0 0.7 convert_bitcast_fusion
  10.7 0.0 copy-start.3
  10.7 0.8 pad_maximum_fusion.kv_ref
  11.5 0.6 pad_maximum_fusion.1.aux_ref
  12.1 12.3 %attention.1 = bf16[320,256]{1,0:T(8,128)(2,1)} custom-call(bf16[320,256]{1,0:T(8,128)(2,1)} %q_ref.1, f32[320,1]{1,0:T(8,128)} %broadcast_in_dim.12.qdoc_ref, bf16[2,320,256]{2,1,0:T(8,128)(2,1)} %pad_maximum_fusion.kv_ref, f32[8,320]{1,0:T(8,128)} %pad_maximum_fusion.1.aux_ref), custom_call_target="tpu_custom_call" | custom-call | tf_op jit(solution)/shard_map/attention/pallas_call | solution.py:195
  24.4 0.0 copy-done
  24.4 2.5 convolution_convert_fusion
  26.9 0.0 reduce-scatter.3.cloned.1.call-update
  26.9 0.0 all-gather.2.cloned.1.call-start
  27.0 0.0 copy-done.4
  27.0 0.1 copy.19
  27.1 0.1 eq.29
  27.3 0.1 eq.25
  27.4 1.4 reduce-window.6
  28.8 0.1 slice.26
  28.9 0.1 copy.21
  29.1 0.2 reduce-window.9
  29.2 0.1 copy.22
  29.3 0.1 copy.18
  29.4 0.1 mul.60
  29.6 0.1 fusion.16
  29.7 43.2 %reduce-scatter.3.cloned.1.call-done = bf16[320,512]{1,0:T(8,128)(2,1)} async-done(((bf16[320,2048]{1,0:T(8,128)(2,1)}), bf16[320,512]{1,0:T(8,128)(2,1)}) %reduce-scatter.3.cloned.1.call-update) | async-done | bytes 327696 | tf_op jit(solution)/shard_map/reduce_scatter | solution.py:233
  72.9 0.0 copy-done.3
  72.9 1.1 add_convert_fusion.1
  74.0 0.3 broadcast_in_dim.11
  74.3 1.1 reshape.118
  75.4 6.5 %scatter_custom_fusion = bf16[856,512]{1,0:T(8,128)(2,1)S(1)} fusion(s32[640]{0:T(1024)S(1)} %fusion.18, bf16[640,512]{1,0:T(8,128)(2,1)} %reshape.118, bf16[]{:T(256)} %constant.9.clone.1), kind=kCustom, calls=%fused_computation.19 | custom fusion | bytes 877056 | tf_op jit(solution)/shard_map/scatter | solution.py:247
  81.9 0.3 reshape.102
  82.2 0.0 copy-start.5
  82.2 28.6 %all_to_all.10 = bf16[8,107,512]{2,1,0:T(8,128)(2,1)} all-to-all(bf16[8,107,512]{2,1,0:T(8,128)(2,1)S(1)} %reshape.102), channel_id=1, replica_groups=mesh['sp'=8,'tp'=4] {'sp'}, dimensions={0} | all-to-all | bytes 1753088 | tf_op jit(solution)/shard_map/all_to_all | solution.py:249
  110.7 0.0 all-gather.2.cloned.1.call-update
  110.8 0.3 reduce-scatter.5.cloned.1.call-start
  111.0 29.1 %all-gather.2.cloned.1.call-done = bf16[8,107,2048]{2,1,0:T(8,128)(2,1)} async-done(((bf16[8,107,512]{2,1,0:T(8,128)(2,1)}), bf16[8,107,2048]{2,1,0:T(8,128)(2,1)}) %all-gather.2.cloned.1.call-update) | async-done | bytes 3506192 | tf_op jit(solution)/shard_map/all_gather | solution.py:250
  140.1 0.0 copy-start.1
  140.1 3.0 %fusion = f32[8,107]{1,0:T(8,128)S(1)} fusion(bf16[8,107,2048]{2,1,0:T(8,128)(2,1)} %all-gather.2.cloned.1.call-done), kind=kLoop, calls=%fused_computation.4 | loop fusion | flops 5258408 | bytes 3509600 | tf_op jit(solution)/shard_map/reduce_sum | solution.py:253
  143.1 0.0 copy-done.5
  143.1 0.1 copy-done.1
  143.2 2.7 %fusion.2 = bf16[8,107,2048]{2,1,0:T(8,128)(2,1)} fusion(bf16[8,107,2048]{2,1,0:T(8,128)(2,1)S(1)} %copy-done.1, f32[2048]{0:T(1024)S(1)} %copy-done.5, f32[8,107]{1,0:T(8,128)S(1)} %add_rsqrt_fusion), kind=kLoop, calls=%fused_computation.6 | loop fusion | flops 7012352 | bytes 7023968 | tf_op jit(solution)/shard_map/convert_element_type | solution.py:254
  145.9 4.9 %convert_element_type.71 = bf16[856,2048]{1,0:T(8,128)(2,1)} reshape(bf16[8,107,2048]{2,1,0:T(8,128)(2,1)} %fusion.2) | data formatting | bytes 7012352 | tf_op jit(solution)/shard_map/convert_element_type | solution.py:254
  150.8 7.0 %fusion.5 = f32[856,896]{1,0:T(8,128)S(1)} fusion(bf16[856,2048]{1,0:T(8,128)(2,1)} %convert_element_type.71, bf16[1,2048,896]{2,1,0:T(8,128)(2,1)} %param.24), kind=kOutput, calls=%fused_computation.9 | convolution fusion | flops 3141533696 | bytes 10244096 | tf_op jit(solution)/shard_map/dot_general | solution.py:258
  157.9 0.0 copy-done.2
  157.9 0.0 copy-done.7
  157.9 0.0 copy-start.8
  157.9 4.0 %multiply_convert_fusion = bf16[856,896]{1,0:T(8,128)(2,1)S(1)} fusion(f32[856,896]{1,0:T(8,128)S(1)} %fusion.5, bf16[856,2048]{1,0:T(8,128)(2,1)S(1)} %copy-done.2, bf16[1,2048,896]{2,1,0:T(8,128)(2,1)S(1)} %copy-done.7), kind=kOutput, calls=%fused_computation.14 | convolution fusion | flops 3146135552 | bytes 11778048 | tf_op jit(solution)/shard_map/dot_general | solution.py:257
  161.9 0.0 copy-done.8
  161.9 5.3 %fusion.9 = bf16[856,2048]{1,0:T(8,128)(2,1)} fusion(bf16[856,896]{1,0:T(8,128)(2,1)S(1)} %multiply_convert_fusion, bf16[1,896,2048]{2,1,0:T(8,128)(2,1)S(1)} %copy-done.8), kind=kOutput, calls=%fused_computation.13 | convolution fusion | flops 3143286784 | bytes 8710144 | tf_op jit(solution)/shard_map/dot_general | solution.py:260
  167.2 0.0 reduce-scatter.5.cloned.1.call-update
  167.2 40.2 %reduce-scatter.5.cloned.1.call-done = bf16[856,512]{1,0:T(8,128)(2,1)} async-done(((bf16[856,2048]{1,0:T(8,128)(2,1)}), bf16[856,512]{1,0:T(8,128)(2,1)}) %reduce-scatter.5.cloned.1.call-update) | async-done | bytes 876560 | tf_op jit(solution)/shard_map/reduce_scatter | solution.py:261
  207.4 2.4 reshape.103
  209.8 5.5 %all-to-all-start.1 = ((bf16[8,107,512]{2,1,0:T(8,128)(2,1)}), bf16[8,107,512]{2,1,0:T(8,128)(2,1)S(1)}, u32[]{:S(2)}, u32[]{:S(2)}) async-start(bf16[8,107,512]{2,1,0:T(8,128)(2,1)} %reshape.103), calls=%async_computation.3 | async-start | bytes 1835008 | tf_op jit(solution)/shard_map/all_to_all | solution.py:265
  215.3 0.0 copy-done.6
  215.3 0.1 copy.23
  215.5 22.8 %all-to-all-done.1 = bf16[8,107,512]{2,1,0:T(8,128)(2,1)S(1)} async-done(((bf16[8,107,512]{2,1,0:T(8,128)(2,1)}), bf16[8,107,512]{2,1,0:T(8,128)(2,1)S(1)}, u32[]{:S(2)}, u32[]{:S(2)}) %all-to-all-start.1) | async-done | bytes 876576 | tf_op jit(solution)/shard_map/all_to_all | solution.py:265
  238.2 0.3 reshape.104
  238.5 3.3 %gather_fusion = bf16[640,512]{1,0:T(8,128)(2,1)} fusion(bf16[856,512]{1,0:T(8,128)(2,1)S(1)} %reshape.104, s32[1024]{0:T(1024)S(1)} %pad_clamp_fusion), kind=kCustom, calls=%fused_computation | custom fusion | bytes 1313280 | tf_op jit(solution)/shard_map/gather | solution.py:266
  241.8 2.0 reshape.105
  243.8 1.6 multiply_reduce_fusion
  245.4 0.8 add_convert_fusion
  (11 shorter events, 0.1 us)
Async XLA Ops:
  6.5 17.9 %copy-start = (bf16[256,2048]{1,0:T(8,128)(2,1)S(1)}, bf16[256,2048]{1,0:T(8,128)(2,1)}, u32[]{:S(2)}) copy-start(bf16[256,2048]{1,0:T(8,128)(2,1)} %param.18) | copy-start | bytes 3145732
  6.5 20.4 %copy-start.4 = (s32[320,2]{0,1:T(2,128)S(1)}, s32[320,2]{0,1:T(2,128)}, u32[]{:S(2)}) copy-start(s32[320,2]{0,1:T(2,128)} %param.21) | copy-start | bytes 7684
  6.5 66.4 %reduce-scatter.3.cloned.1.call-start = ((), (), s32[]{:S(2)}) async-start(), calls=%async_computation.4 | async-start | bytes 1638400 | tf_op jit(solution)/shard_map/reduce_scatter | solution.py:233
  10.7 62.2 %copy-start.3 = (bf16[320,512]{1,0:T(8,128)(2,1)S(1)}, bf16[320,512]{1,0:T(8,128)(2,1)}, u32[]{:S(2)}) copy-start(bf16[320,512]{1,0:T(8,128)(2,1)} %param.19) | copy-start | bytes 983044
  26.9 113.2 %all-gather.2.cloned.1.call-start = ((), (), s32[]{:S(2)}) async-start(), calls=%async_computation.5 | async-start | bytes 4587520 | tf_op jit(solution)/shard_map/all_gather | solution.py:250
  82.2 61.0 %copy-start.5 = (f32[2048]{0:T(1024)S(1)}, f32[2048]{0:T(1024)}, u32[]{:S(2)}) copy-start(f32[2048]{0:T(1024)} %param.20) | copy-start | bytes 24580
  110.8 96.7 %reduce-scatter.5.cloned.1.call-start = ((), (), s32[]{:S(2)}) async-start(), calls=%async_computation.6 | async-start | bytes 4382720 | tf_op jit(solution)/shard_map/reduce_scatter | solution.py:261
  140.1 3.1 %copy-start.1 = (bf16[8,107,2048]{2,1,0:T(8,128)(2,1)S(1)}, bf16[8,107,2048]{2,1,0:T(8,128)(2,1)}, u32[]{:S(2)}) copy-start(bf16[8,107,2048]{2,1,0:T(8,128)(2,1)} %all-gather.2.cloned.1.call-done) | copy-start | bytes 10518532
  150.8 7.0 %copy-start.2 = (bf16[856,2048]{1,0:T(8,128)(2,1)S(1)}, bf16[856,2048]{1,0:T(8,128)(2,1)}, u32[]{:S(2)}) copy-start(bf16[856,2048]{1,0:T(8,128)(2,1)} %convert_element_type.71) | copy-start | bytes 10518532
  150.8 7.0 %copy-start.7 = (bf16[1,2048,896]{2,1,0:T(8,128)(2,1)S(1)}, bf16[1,2048,896]{2,1,0:T(8,128)(2,1)}, u32[]{:S(2)}) copy-start(bf16[1,2048,896]{2,1,0:T(8,128)(2,1)} %param.23) | copy-start | bytes 11010052
  157.9 4.1 %copy-start.8 = (bf16[1,896,2048]{2,1,0:T(8,128)(2,1)S(1)}, bf16[1,896,2048]{2,1,0:T(8,128)(2,1)}, u32[]{:S(2)}) copy-start(bf16[1,896,2048]{2,1,0:T(8,128)(2,1)} %param.25) | copy-start | bytes 11010052
  167.2 48.1 %copy-start.6 = (f32[320,2]{0,1:T(2,128)S(1)}, f32[320,2]{0,1:T(2,128)}, u32[]{:S(2)}) copy-start(f32[320,2]{0,1:T(2,128)} %param.22) | copy-start | bytes 7684
  209.8 28.4 %all-to-all-start.1 = ((bf16[8,107,512]{2,1,0:T(8,128)(2,1)}), bf16[8,107,512]{2,1,0:T(8,128)(2,1)S(1)}, u32[]{:S(2)}, u32[]{:S(2)}) async-start(bf16[8,107,512]{2,1,0:T(8,128)(2,1)} %reshape.103), calls=%async_computation.3 | async-start | bytes 1835008 | tf_op jit(solution)/shard_map/all_to_all | solution.py:265
Sparse Core Ops, SparseCore 0:
  27.0 45.8 reduce-scatter.2
  110.9 29.1 all-gather.1
  167.4 40.0 reduce-scatter.4
where the time goes:
time: 253 us
  waiting for transfers between devices  135 us (53%)
  blocking collectives  28.6 us (11%)
  local copies, waits for them, and re-layouts  25 us (10%)
  matrix products  18.8 us (7%)
  other arithmetic  13.7 us (5%)
  between operations  13.3 us (5%)
  Pallas kernels  12.3 us (5%)
  starting transfers between devices  5.82 us (2%)
    reduce_scatter x1, waiting for transfers between devices, shards(): lax.psum_scatter(partial_value.astype(jnp.bfloat16), 'tp', scatter_dimens...  43.2 us
    reduce_scatter x1, waiting for transfers between devices, shards(): lax.psum_scatter(partial_out.astype(jnp.bfloat16), 'tp', scatter_dimensio...  40.2 us
    all_gather x1, waiting for transfers between devices, shards(): arrived = lax.all_gather(arrived, 'tp', axis=2, tiled=True)  29.1 us
    all_to_all x1, blocking collectives, shards(): lax.all_to_all(buffer, 'sp', split_axis=0, concat_axis=0, tiled=True)  28.6 us
    all_to_all x1, waiting for transfers between devices, shards(): lax.all_to_all(result, 'sp', split_axis=0, concat_axis=0, tiled=True)  22.8 us
    pallas_call x1, Pallas kernels, attend(): pl.pallas_call(functools.partial(attention_kernel, count), out_shape=jax....  12.3 us
    dot_general x1, matrix products, shards(): jnp.dot(row_block, up_weight[0], preferred_element_type=jnp.float32)  7.02 us
    scatter x1, local copies, waits for them, and re-layouts, shards(): buffer = buffer.at[target].set(jnp.repeat(sending, top_count, axis=0))  6.48 us
  transfers between devices with their start and end apart: 4, of which 4 were waited for; matrix products, arithmetic and copies ran while one was open for 1% of the time, Pallas kernels for 0%

commit v1 on v0

--- a/solution.py
+++ b/solution.py
@@ -7,7 +7,6 @@
 from jax.experimental.pallas import tpu as pltpu
 from jax.sharding import PartitionSpec as P
 
-D = 2048
 HEAD = 64
 REACH = 4
 LANES = 128
@@ -212,6 +211,248 @@
     )(query_rows, docs[:, None], key_value, aux)
 
 
+def greet(count, others):
+    me = lax.axis_index("sp")
+    barrier = pltpu.get_barrier_semaphore()
+
+    def signal(r, carry):
+        pl.semaphore_signal(
+            barrier, inc=1, device_id={"sp": lax.rem(me + r, count)}, device_id_type=MESH
+        )
+        return carry
+
+    if count > 1:
+        lax.fori_loop(1, count, signal, 0)
+    for other in others:
+        pl.semaphore_signal(barrier, inc=1, device_id={"tp": other}, device_id_type=MESH)
+    pl.semaphore_wait(barrier, count - 1 + len(others))
+
+
+def each(low, high, body):
+    def step(r, carry):
+        body(r)
+        return carry
+
+    lax.fori_loop(low, high, step, 0)
+
+
+def neighbours():
+    t = lax.axis_index("tp")
+    return t, t + 1 - 2 * lax.rem(t, 2), lax.rem(t + 2, lax.axis_size("tp"))
+
+
+def dispatch_kernel(count, in_ref, gain_ref, out_ref, held, send, recv):
+    me = lax.axis_index("sp")
+    t, partner, across = neighbours()
+    _, capacity, feats = in_ref.shape
+    features = held.shape[2]
+    greet(count, (partner, across))
+
+    def columns(owner):
+        return pl.ds(pl.multiple_of(owner * feats, feats), feats)
+
+    def source(r):
+        return lax.rem(me - r + count, count)
+
+    def arrival(r):
+        target = lax.rem(me + r, count)
+        return pltpu.make_async_remote_copy(
+            src_ref=in_ref.at[target], dst_ref=held.at[me, :, columns(t)],
+            send_sem=send.at[0, r], recv_sem=recv.at[0, r],
+            device_id={"sp": target}, device_id_type=MESH,
+        )
+
+    def share(r, kind, owner, target):
+        place = held.at[source(r), :, columns(owner)]
+        return pltpu.make_async_remote_copy(
+            src_ref=place, dst_ref=place, send_sem=send.at[kind, r], recv_sem=recv.at[kind, r],
+            device_id={"tp": target}, device_id_type=MESH,
+        )
+
+    def cross(r):
+        return share(r, 1, t, across)
+
+    def pair(r):
+        return share(r, 2, t, partner)
+
+    def relay(r):
+        return share(r, 3, across, partner)
+
+    def spread(r):
+        cross(r).start()
+        pair(r).start()
+
+    def norm(r):
+        pair(r).wait_recv()
+        relay(r).wait_recv()
+        row_block = held[source(r)].astype(jnp.float32)
+        square_mean = jnp.sum(row_block * row_block, axis=1, keepdims=True) / features
+        out_ref[source(r)] = (
+            row_block * lax.rsqrt(square_mean + NORM_EPS) * gain_ref[...]
+        ).astype(out_ref.dtype)
+
+    each(1, count, lambda r: arrival(r).start())
+    local = pltpu.make_async_copy(in_ref.at[me], held.at[me, :, columns(t)], send.at[0, 0])
+    local.start()
+    local.wait()
+    spread(0)
+
+    def take(r):
+        arrival(r).wait_recv()
+        spread(r)
+
+    each(1, count, take)
+
+    def forward(r):
+        cross(r).wait_recv()
+        relay(r).start()
+
+    forward(0)
+
+    def finish(r):
+        forward(r)
+        norm(r - 1)
+
+    each(1, count, finish)
+    norm(count - 1)
+    each(1, count, lambda r: arrival(r).wait_send())
+
+    def drain(r):
+        cross(r).wait_send()
+        pair(r).wait_send()
+        relay(r).wait_send()
+
+    each(0, count, drain)
+
+
+def reduce_kernel(count, back, in_ref, out_ref, near, outgoing, far, final, send, recv):
+    me = lax.axis_index("sp")
+    t, partner, across = neighbours()
+    partner_across = lax.rem(partner + 2, lax.axis_size("tp"))
+    blocks, rows, _ = in_ref.shape
+    feats = out_ref.shape[2]
+    greet(count if back else 1, (partner, across))
+
+    def columns(owner):
+        return pl.ds(pl.multiple_of(owner * feats, feats), feats)
+
+    def place(r):
+        return lax.rem(me + r + 1, blocks) if back else r
+
+    def pair(r, which, owner):
+        return pltpu.make_async_remote_copy(
+            src_ref=in_ref.at[place(r), :, columns(owner)], dst_ref=near.at[which, r],
+            send_sem=send.at[which, r], recv_sem=recv.at[which, r],
+            device_id={"tp": partner}, device_id_type=MESH,
+        )
+
+    def cross(r):
+        return pltpu.make_async_remote_copy(
+            src_ref=outgoing.at[r], dst_ref=far.at[r],
+            send_sem=send.at[2, r], recv_sem=recv.at[2, r],
+            device_id={"tp": across}, device_id_type=MESH,
+        )
+
+    def home(r):
+        return pltpu.make_async_remote_copy(
+            src_ref=final.at[r], dst_ref=out_ref.at[me],
+            send_sem=send.at[3, r], recv_sem=recv.at[3, r],
+            device_id={"sp": place(r)}, device_id_type=MESH,
+        )
+
+    def start_pair(r):
+        pair(r, 0, partner_across).start()
+        pair(r, 1, partner).start()
+
+    each(0, blocks, start_pair)
+
+    def halve(r):
+        pair(r, 0, partner_across).wait_recv()
+        outgoing[r] = (
+            in_ref[place(r), :, columns(across)].astype(jnp.float32)
+            + near[0, r].astype(jnp.float32)
+        ).astype(outgoing.dtype)
+        cross(r).start()
+
+    each(0, blocks, halve)
+
+    def total(r):
+        pair(r, 1, partner).wait_recv()
+        cross(r).wait_recv()
+        return (
+            in_ref[place(r), :, columns(t)].astype(jnp.float32)
+            + near[1, r].astype(jnp.float32)
+            + far[r].astype(jnp.float32)
+        ).astype(out_ref.dtype)
+
+    def drain(r):
+        pair(r, 0, partner_across).wait_send()
+        pair(r, 1, partner).wait_send()
+        cross(r).wait_send()
+
+    if back:
+        def finish(r):
+            final[r] = total(r)
+            home(r).start()
+
+        each(0, blocks - 1, finish)
+        out_ref[me] = total(blocks - 1)
+
+        def collect(r):
+            home(r).wait_recv()
+            home(r).wait_send()
+
+        each(0, blocks - 1, collect)
+    else:
+        def finish(r):
+            out_ref[r] = total(r)
+
+        each(0, blocks, finish)
+    each(0, blocks, drain)
+
+
+def dispatch(blocks, norm_gain):
+    count, capacity, feats = blocks.shape
+    features = norm_gain.shape[0]
+    vmem = pl.BlockSpec(memory_space=pltpu.VMEM)
+    return pl.pallas_call(
+        functools.partial(dispatch_kernel, count),
+        out_shape=jax.ShapeDtypeStruct((count, capacity, features), jnp.bfloat16),
+        in_specs=[vmem] * 2,
+        out_specs=vmem,
+        scratch_shapes=[
+            pltpu.VMEM((count, capacity, features), jnp.bfloat16),
+            pltpu.SemaphoreType.DMA((4, count)),
+            pltpu.SemaphoreType.DMA((4, count)),
+        ],
+        compiler_params=pltpu.CompilerParams(collective_id=1, has_side_effects=True),
+        name="dispatch",
+    )(blocks, norm_gain[None, :])
+
+
+def reduce_tp(partial, back, collective_id):
+    blocks, rows, features = partial.shape
+    feats = features // lax.axis_size("tp")
+    vmem = pl.BlockSpec(memory_space=pltpu.VMEM)
+    slots = pltpu.VMEM((blocks, rows, feats), jnp.bfloat16)
+    return pl.pallas_call(
+        functools.partial(reduce_kernel, lax.axis_size("sp"), back),
+        out_shape=jax.ShapeDtypeStruct((blocks, rows, feats), jnp.bfloat16),
+        in_specs=[vmem],
+        out_specs=vmem,
+        scratch_shapes=[
+            pltpu.VMEM((2, blocks, rows, feats), jnp.bfloat16),
+            slots,
+            slots,
+            slots if back else pltpu.VMEM((8, 128), jnp.bfloat16),
+            pltpu.SemaphoreType.DMA((4, blocks)),
+            pltpu.SemaphoreType.DMA((4, blocks)),
+        ],
+        compiler_params=pltpu.CompilerParams(collective_id=collective_id, has_side_effects=True),
+        name="combine" if back else "project",
+    )(partial)
+
+
 def shards(
     query_rows,
     key_rows,
@@ -229,48 +470,44 @@
 ):
     portion_rows = query_rows.shape[0]
     attended = attend(query_rows, key_rows, value_rows, key_shift, documents)
-    partial_value = jnp.dot(attended, out_weight, preferred_element_type=jnp.float32)
-    projected = lax.psum_scatter(
-        partial_value.astype(jnp.bfloat16), "tp", scatter_dimension=1, tiled=True
-    ).astype(jnp.float32)
-    middle = (stream.astype(jnp.float32) + projected).astype(jnp.bfloat16)
-    middle_wide = middle.astype(jnp.float32)
-    sending = middle
+    partial_value = jnp.dot(attended, out_weight, preferred_element_type=jnp.float32).astype(
+        jnp.bfloat16
+    )
+    cuts = 4 if portion_rows % 64 == 0 else 1
+    projected = reduce_tp(
+        partial_value.reshape(cuts, portion_rows // cuts, partial_value.shape[1]), False, 2
+    ).reshape(portion_rows, stream.shape[1])
+    middle = (stream.astype(jnp.float32) + projected.astype(jnp.float32)).astype(jnp.bfloat16)
     top_count = expert_ids.shape[1]
     experts = lax.axis_size("sp") * gate_weight.shape[0]
     capacity = (4 * portion_rows * top_count + 3 * experts - 1) // (3 * experts)
+    capacity = (capacity + 15) // 16 * 16
     flat_ids = expert_ids.reshape(portion_rows * top_count)
     onehot = (flat_ids[:, None] == jnp.arange(experts, dtype=jnp.int32)[None, :]).astype(jnp.int32)
     slot_index = jnp.sum((jnp.cumsum(onehot, axis=0) - 1) * onehot, axis=1)
-    target = flat_ids * capacity + slot_index
-    buffer = jnp.zeros((experts * capacity, sending.shape[1]), jnp.bfloat16)
-    buffer = buffer.at[target].set(jnp.repeat(sending, top_count, axis=0))
-    buffer = buffer.reshape(experts, capacity, sending.shape[1])
-    arrived = lax.all_to_all(buffer, "sp", split_axis=0, concat_axis=0, tiled=True)
-    arrived = lax.all_gather(arrived, "tp", axis=2, tiled=True)
-    sources, item_count, feat_count = arrived.shape
-    row_block = arrived.reshape(sources * item_count, feat_count).astype(jnp.float32)
-    square_mean = jnp.sum(row_block * row_block, axis=1, keepdims=True) / D
-    row_block = (row_block * lax.rsqrt(square_mean + NORM_EPS) * norm_gain[None, :]).astype(
-        jnp.bfloat16
-    )
+    target = (flat_ids * capacity + slot_index).reshape(portion_rows, top_count)
+    slots = jnp.arange(experts * capacity, dtype=jnp.int32)
+    placed = target[:, 0][None, :] == slots[:, None]
+    for k in range(1, top_count):
+        placed = placed | (target[:, k][None, :] == slots[:, None])
+    blocks = jnp.dot(
+        placed.astype(jnp.bfloat16), middle, preferred_element_type=jnp.float32
+    ).astype(jnp.bfloat16)
+    arrived = dispatch(blocks.reshape(experts, capacity, middle.shape[1]), norm_gain)
+    row_block = arrived.reshape(experts * capacity, arrived.shape[2])
     gate_value = jnp.dot(row_block, gate_weight[0], preferred_element_type=jnp.float32)
     up_value = jnp.dot(row_block, up_weight[0], preferred_element_type=jnp.float32)
     hidden = (jax.nn.silu(gate_value) * up_value).astype(jnp.bfloat16)
     partial_out = jnp.dot(hidden, down_weight[0], preferred_element_type=jnp.float32)
-    summed = lax.psum_scatter(
-        partial_out.astype(jnp.bfloat16), "tp", scatter_dimension=1, tiled=True
-    ).astype(jnp.float32)
-    result = summed.astype(jnp.bfloat16).reshape(sources, item_count, summed.shape[1])
-    returned_rows = lax.all_to_all(result, "sp", split_axis=0, concat_axis=0, tiled=True)
-    picked = returned_rows.reshape(experts * capacity, returned_rows.shape[2])[target].astype(
-        jnp.float32
-    )
-    mixed = jnp.sum(
-        picked.reshape(portion_rows, top_count, picked.shape[1]) * expert_weights[:, :, None],
-        axis=1,
-    )
-    return (middle_wide + mixed).astype(jnp.bfloat16)
+    returned = reduce_tp(
+        partial_out.astype(jnp.bfloat16).reshape(experts, capacity, partial_out.shape[1]), True, 3
+    ).reshape(experts * capacity, middle.shape[1])
+    result = middle.astype(jnp.float32)
+    for k in range(top_count):
+        chosen = (target[:, k][:, None] == slots[None, :]).astype(jnp.bfloat16)
+        picked = jnp.dot(chosen, returned, preferred_element_type=jnp.float32)
+        result = result + picked * expert_weights[:, k][:, None]
+    return result.astype(jnp.bfloat16)
 
 
 def solution(mesh):

time: 253 us -> 154 us (0.61)
  waiting for transfers between devices: 135 us -> 0 us
  Pallas kernels: 12.3 us -> 119 us
  blocking collectives: 28.6 us -> 0 us
  local copies, waits for them, and re-layouts: 25 us -> 3.78 us
  between operations: 13.3 us -> 0.21 us
  other arithmetic: 13.7 us -> 5.53 us
  matrix products: 18.8 us -> 25.1 us
  starting transfers between devices: 5.82 us -> 0 us
    pallas_call x0 -> x3, Pallas kernels: none -> 107 us  [the longest x1 55.5 us: dispatch(): pl.pallas_call(functools.partial(dispatch_kernel, count), out_shape=jax.S...]
    reduce_scatter x2 -> x0, waiting for transfers between devices: 83.4 us -> none  [the longest x1 43.2 us: shards(): lax.psum_scatter(partial_value.astype(jnp.bfloat16), 'tp', scatter_dimens...]
    all_gather x1 -> x0, waiting for transfers between devices: 29.1 us -> none  [shards(): arrived = lax.all_gather(arrived, 'tp', axis=2, tiled=True)]
    all_to_all x1 -> x0, blocking collectives: 28.6 us -> none  [shards(): lax.all_to_all(buffer, 'sp', split_axis=0, concat_axis=0, tiled=True)]
    all_to_all x1 -> x0, waiting for transfers between devices: 22.8 us -> none  [shards(): lax.all_to_all(result, 'sp', split_axis=0, concat_axis=0, tiled=True)]
    convert_element_type x2 -> x0, local copies, waits for them, and re-layouts: 6.86 us -> none  [the longest x1 4.88 us: shards(): (row_block * lax.rsqrt(square_mean + NORM_EPS) * norm_gain[None, :]).asty...]
    scatter x1 -> x0, local copies, waits for them, and re-layouts: 6.48 us -> none  [shards(): buffer = buffer.at[target].set(jnp.repeat(sending, top_count, axis=0))]
    dot_general x0 -> x3, matrix products: none -> 5.77 us  [the longest x2 4.19 us: shards(): picked = jnp.dot(chosen, returned, preferred_element_type=jnp.float32)]
  transfers between devices with their start and end apart: 4 -> 0, of which waited for: 4 -> 0; matrix products, arithmetic and copies ran while one was open for 1% -> 0% of each run, Pallas kernels for 0% -> 0%
where the time goes in v1:
time: 154 us
  Pallas kernels  119 us (77%)
  matrix products  25.1 us (16%)
  other arithmetic  5.53 us (4%)
  local copies, waits for them, and re-layouts  3.78 us (2%)
    pallas_call x1, Pallas kernels, dispatch(): pl.pallas_call(functools.partial(dispatch_kernel, count), out_shape=jax.S...  55.5 us
    pallas_call x2, Pallas kernels, reduce_tp(): pl.pallas_call(functools.partial(reduce_kernel, lax.axis_size('sp'), back...  51.2 us
    pallas_call x1, Pallas kernels, attend(): pl.pallas_call(functools.partial(attention_kernel, count), out_shape=jax....  12.3 us
    dot_general x1, matrix products, shards(): jnp.dot(row_block, up_weight[0], preferred_element_type=jnp.float32)  7.23 us
    dot_general x1, matrix products, shards(): jnp.dot(hidden, down_weight[0], preferred_element_type=jnp.float32)  5.43 us
    dot_general x1, matrix products, shards(): jnp.dot(row_block, gate_weight[0], preferred_element_type=jnp.float32)  4.2 us
    dot_general x2, matrix products, shards(): picked = jnp.dot(chosen, returned, preferred_element_type=jnp.float32)  4.19 us

profile of v1, /device:TPU:0, one launch (start us, length us, event | category | flops | bytes accessed | tf_op | source)
XLA Modules:
  0.0 153.7 jit_solution(4273757864077717590)
XLA Ops:
  0.0 0.0 copy-start
  0.0 1.0 fusion.23
  1.0 0.9 fusion.24
  2.0 0.0 copy-start.2
  2.0 0.8 pad_maximum_fusion.kv_ref
  2.8 0.0 copy-start.3
  2.8 0.7 convert_element_type.48
  3.5 0.8 broadcast_in_dim.9.qdoc_ref
  4.3 0.7 convert_bitcast_fusion
  4.9 0.6 pad_maximum_fusion.1.aux_ref
  5.6 12.3 %attention.1 = bf16[320,256]{1,0:T(8,128)(2,1)} custom-call(bf16[320,256]{1,0:T(8,128)(2,1)} %q_ref.1, f32[320,1]{1,0:T(8,128)} %broadcast_in_dim.9.qdoc_ref, bf16[2,320,256]{2,1,0:T(8,128)(2,1)} %pad_maximum_fusion.kv_ref, f32[8,320]{1,0:T(8,128)} %pad_maximum_fusion.1.aux_ref), custom_call_target="tpu_custom_call" | custom-call | tf_op jit(solution)/shard_map/attention/pallas_call | solution.py:194
  17.9 0.0 copy-done
  17.9 2.5 %convolution_convert_fusion = bf16[320,2048]{1,0:T(8,128)(2,1)} fusion(bf16[320,256]{1,0:T(8,128)(2,1)} %attention.1, bf16[256,2048]{1,0:T(8,128)(2,1)S(1)} %copy-done), kind=kOutput, calls=%fused_computation.8 | convolution fusion | flops 336199680 | bytes 2523136 | tf_op jit(solution)/shard_map/dot_general | solution.py:473
  20.4 13.6 %project.1 = bf16[4,80,512]{2,1,0:T(8,128)(2,1)} custom-call(bf16[4,80,2048]{2,1,0:T(8,128)(2,1)} %bitcast.44), custom_call_target="tpu_custom_call" | custom-call | tf_op jit(solution)/shard_map/project/pallas_call | solution.py:438
  34.0 0.0 copy-done.2
  34.0 1.1 fusion.18
  35.1 0.0 copy-done.3
  35.1 0.1 copy.31
  35.2 0.1 eq.85
  35.4 1.4 reduce-window.6
  36.8 0.1 slice.42
  36.9 0.1 copy.33
  37.0 0.2 reduce-window.9
  37.2 0.1 copy.34
  37.3 0.1 eq.81
  37.4 0.1 fusion.21
  37.5 0.1 reduce_sum.12
  37.6 0.1 copy.35
  37.8 1.6 %convolution_convert_fusion.1 = bf16[896,512]{1,0:T(8,128)(2,1)} fusion(bf16[320,512]{1,0:T(8,128)(2,1)S(1)} %fusion.18, s32[320]{0:T(512)S(1)} %get-tuple-element.8, s32[320]{0:T(512)S(1)} %get-tuple-element.7), kind=kOutput, calls=%fused_computation.9 | convolution fusion | flops 294920192 | bytes 1247744 | tf_op jit(solution)/shard_map/dot_general | solution.py:493
  39.4 55.5 %dispatch.1 = bf16[8,112,2048]{2,1,0:T(8,128)(2,1)} custom-call(bf16[8,112,512]{2,1,0:T(8,128)(2,1)} %bitcast.50, f32[1,2048]{1,0:T(1,128)} %bitcast.53), custom_call_target="tpu_custom_call" | custom-call | tf_op jit(solution)/shard_map/dispatch/pallas_call | solution.py:418
  94.9 0.0 copy-start.1
  94.9 0.0 copy-start.5
  95.0 7.2 %fusion.2 = f32[896,896]{1,0:T(8,128)S(1)} fusion(bf16[896,2048]{1,0:T(8,128)(2,1)} %bitcast.45, bf16[1,2048,896]{2,1,0:T(8,128)(2,1)} %param.24), kind=kOutput, calls=%fused_computation.2 | convolution fusion | flops 3288334336 | bytes 10551296 | tf_op jit(solution)/shard_map/dot_general | solution.py:499
  102.2 0.0 copy-done.1
  102.2 0.0 copy-done.5
  102.2 0.0 copy-start.6
  102.2 4.2 %multiply_convert_fusion = bf16[896,896]{1,0:T(8,128)(2,1)S(1)} fusion(f32[896,896]{1,0:T(8,128)S(1)} %fusion.2, bf16[896,2048]{1,0:T(8,128)(2,1)S(1)} %bitcast.46, bf16[1,2048,896]{2,1,0:T(8,128)(2,1)S(1)} %copy-done.5), kind=kOutput, calls=%fused_computation.7 | convolution fusion | flops 3293151232 | bytes 12156928 | tf_op jit(solution)/shard_map/dot_general | solution.py:498
  106.4 0.0 copy-done.6
  106.4 5.4 %fusion.6 = bf16[896,2048]{1,0:T(8,128)(2,1)} fusion(bf16[896,896]{1,0:T(8,128)(2,1)S(1)} %multiply_convert_fusion, bf16[1,896,2048]{2,1,0:T(8,128)(2,1)S(1)} %copy-done.6), kind=kOutput, calls=%fused_computation.6 | convolution fusion | flops 3290169344 | bytes 8945664 | tf_op jit(solution)/shard_map/dot_general | solution.py:501
  111.9 0.0 copy-start.4
  111.9 37.6 %combine.1 = bf16[8,112,512]{2,1,0:T(8,128)(2,1)} custom-call(bf16[8,112,2048]{2,1,0:T(8,128)(2,1)} %bitcast.47), custom_call_target="tpu_custom_call" | custom-call | tf_op jit(solution)/shard_map/combine/pallas_call | solution.py:438
  149.5 0.0 copy-done.4
  149.5 1.7 %fusion.14 = f32[320,512]{1,0:T(8,128)S(1)} fusion(bf16[896,512]{1,0:T(8,128)(2,1)} %bitcast.48, bf16[320,512]{1,0:T(8,128)(2,1)S(1)} %fusion.18, s32[320]{0:T(512)S(1)} %get-tuple-element.7, f32[320]{0:T(512)S(1)} %get-tuple-element.6), kind=kOutput, calls=%fused_computation.16 | convolution fusion | flops 294379520 | bytes 1903104 | tf_op jit(solution)/shard_map/dot_general | solution.py:508
  151.2 2.5 %fusion.15 = bf16[320,512]{1,0:T(8,128)(2,1)} fusion(f32[320,512]{1,0:T(8,128)S(1)} %fusion.14, bf16[896,512]{1,0:T(8,128)(2,1)} %bitcast.49, s32[320]{0:T(512)S(1)} %get-tuple-element.8, f32[320]{0:T(512)S(1)} %get-tuple-element.5), kind=kOutput, calls=%fused_computation.17 | convolution fusion | flops 294379520 | bytes 1903104 | tf_op jit(solution)/shard_map/dot_general | solution.py:508
  (6 shorter events, 0.1 us)
Async XLA Ops:
  0.0 17.9 %copy-start = (bf16[256,2048]{1,0:T(8,128)(2,1)S(1)}, bf16[256,2048]{1,0:T(8,128)(2,1)}, u32[]{:S(2)}) copy-start(bf16[256,2048]{1,0:T(8,128)(2,1)} %param.18) | copy-start | bytes 3145732
  2.0 32.0 %copy-start.2 = (bf16[320,512]{1,0:T(8,128)(2,1)S(1)}, bf16[320,512]{1,0:T(8,128)(2,1)}, u32[]{:S(2)}) copy-start(bf16[320,512]{1,0:T(8,128)(2,1)} %param.19) | copy-start | bytes 983044
  2.8 32.3 %copy-start.3 = (s32[320,2]{0,1:T(2,128)S(1)}, s32[320,2]{0,1:T(2,128)}, u32[]{:S(2)}) copy-start(s32[320,2]{0,1:T(2,128)} %param.21) | copy-start | bytes 7684
  94.9 7.3 %copy-start.1 = (bf16[8,112,2048]{2,1,0:T(8,128)(2,1)S(1)}, bf16[8,112,2048]{2,1,0:T(8,128)(2,1)}, u32[]{:S(2)}) copy-start(bf16[8,112,2048]{2,1,0:T(8,128)(2,1)} %dispatch.1) | copy-start | bytes 11010052
  94.9 7.3 %copy-start.5 = (bf16[1,2048,896]{2,1,0:T(8,128)(2,1)S(1)}, bf16[1,2048,896]{2,1,0:T(8,128)(2,1)}, u32[]{:S(2)}) copy-start(bf16[1,2048,896]{2,1,0:T(8,128)(2,1)} %param.23) | copy-start | bytes 11010052
  102.2 4.2 %copy-start.6 = (bf16[1,896,2048]{2,1,0:T(8,128)(2,1)S(1)}, bf16[1,896,2048]{2,1,0:T(8,128)(2,1)}, u32[]{:S(2)}) copy-start(bf16[1,896,2048]{2,1,0:T(8,128)(2,1)} %param.25) | copy-start | bytes 11010052
  111.9 37.6 %copy-start.4 = (f32[320,2]{0,1:T(2,128)S(1)}, f32[320,2]{0,1:T(2,128)}, u32[]{:S(2)}) copy-start(f32[320,2]{0,1:T(2,128)} %param.22) | copy-start | bytes 7684

commit v2 on v1

--- a/solution.py
+++ b/solution.py
@@ -236,6 +236,15 @@
     lax.fori_loop(low, high, step, 0)
 
 
+def mate(me, r, count):
+    assert count & (count - 1) == 0
+    other, bit = 0, 1
+    while bit < count:
+        other = other + bit * lax.rem(lax.div(me, bit) + lax.div(r, bit), 2)
+        bit *= 2
+    return other
+
+
 def neighbours():
     t = lax.axis_index("tp")
     return t, t + 1 - 2 * lax.rem(t, 2), lax.rem(t + 2, lax.axis_size("tp"))
@@ -252,10 +261,10 @@
         return pl.ds(pl.multiple_of(owner * feats, feats), feats)
 
     def source(r):
-        return lax.rem(me - r + count, count)
+        return mate(me, jnp.int32(r), count)
 
     def arrival(r):
-        target = lax.rem(me + r, count)
+        target = source(r)
         return pltpu.make_async_remote_copy(
             src_ref=in_ref.at[target], dst_ref=held.at[me, :, columns(t)],
             send_sem=send.at[0, r], recv_sem=recv.at[0, r],
@@ -337,7 +346,7 @@
         return pl.ds(pl.multiple_of(owner * feats, feats), feats)
 
     def place(r):
-        return lax.rem(me + r + 1, blocks) if back else r
+        return mate(me, jnp.int32(blocks - 1 - r), blocks) if back else r
 
     def pair(r, which, owner):
         return pltpu.make_async_remote_copy(

time: 154 us -> 147 us (0.955)
  Pallas kernels: 119 us -> 112 us
    pallas_call x2, Pallas kernels: 51.2 us -> 46.6 us  [reduce_tp(): pl.pallas_call(functools.partial(reduce_kernel, lax.axis_size('sp'), back...]
    pallas_call x1, Pallas kernels: 55.5 us -> 52.8 us  [dispatch(): pl.pallas_call(functools.partial(dispatch_kernel, count), out_shape=jax.S...]
where the time goes in v2:
time: 147 us; the launch traced here: 146 us
  Pallas kernels  112 us (76%)
  matrix products  25.1 us (17%)
  other arithmetic  5.53 us (4%)
  local copies, waits for them, and re-layouts  3.78 us (3%)
    pallas_call x1, Pallas kernels, dispatch(): pl.pallas_call(functools.partial(dispatch_kernel, count), out_shape=jax.S...  52.8 us
    pallas_call x2, Pallas kernels, reduce_tp(): pl.pallas_call(functools.partial(reduce_kernel, lax.axis_size('sp'), back...  46.6 us
    pallas_call x1, Pallas kernels, attend(): pl.pallas_call(functools.partial(attention_kernel, count), out_shape=jax....  12.3 us
    dot_general x1, matrix products, shards(): jnp.dot(row_block, up_weight[0], preferred_element_type=jnp.float32)  7.23 us
    dot_general x1, matrix products, shards(): jnp.dot(hidden, down_weight[0], preferred_element_type=jnp.float32)  5.43 us
    dot_general x1, matrix products, shards(): jnp.dot(row_block, gate_weight[0], preferred_element_type=jnp.float32)  4.2 us
    dot_general x2, matrix products, shards(): picked = jnp.dot(chosen, returned, preferred_element_type=jnp.float32)  4.19 us

profile of v2, /device:TPU:0, one launch (start us, length us, event | category | flops | bytes accessed | tf_op | source)
XLA Modules:
  0.0 146.3 jit_solution(1412840329569887486)
XLA Ops:
  0.0 0.0 copy-start
  0.0 1.0 fusion.23
  1.0 0.9 fusion.24
  2.0 0.0 copy-start.2
  2.0 0.8 pad_maximum_fusion.kv_ref
  2.8 0.0 copy-start.3
  2.8 0.7 convert_element_type.48
  3.5 0.8 broadcast_in_dim.9.qdoc_ref
  4.3 0.7 convert_bitcast_fusion
  4.9 0.6 pad_maximum_fusion.1.aux_ref
  5.6 12.3 %attention.1 = bf16[320,256]{1,0:T(8,128)(2,1)} custom-call(bf16[320,256]{1,0:T(8,128)(2,1)} %q_ref.1, f32[320,1]{1,0:T(8,128)} %broadcast_in_dim.9.qdoc_ref, bf16[2,320,256]{2,1,0:T(8,128)(2,1)} %pad_maximum_fusion.kv_ref, f32[8,320]{1,0:T(8,128)} %pad_maximum_fusion.1.aux_ref), custom_call_target="tpu_custom_call" | custom-call | tf_op jit(solution)/shard_map/attention/pallas_call | solution.py:194
  17.9 0.0 copy-done
  17.9 2.5 %convolution_convert_fusion = bf16[320,2048]{1,0:T(8,128)(2,1)} fusion(bf16[320,256]{1,0:T(8,128)(2,1)} %attention.1, bf16[256,2048]{1,0:T(8,128)(2,1)S(1)} %copy-done), kind=kOutput, calls=%fused_computation.8 | convolution fusion | flops 336199680 | bytes 2523136 | tf_op jit(solution)/shard_map/dot_general | solution.py:482
  20.4 13.6 %project.1 = bf16[4,80,512]{2,1,0:T(8,128)(2,1)} custom-call(bf16[4,80,2048]{2,1,0:T(8,128)(2,1)} %bitcast.44), custom_call_target="tpu_custom_call" | custom-call | tf_op jit(solution)/shard_map/project/pallas_call | solution.py:447
  34.0 0.0 copy-done.2
  34.0 1.1 fusion.18
  35.1 0.0 copy-done.3
  35.1 0.1 copy.31
  35.2 0.1 eq.85
  35.4 1.4 reduce-window.6
  36.8 0.1 slice.42
  36.9 0.1 copy.33
  37.0 0.2 reduce-window.9
  37.2 0.1 copy.34
  37.3 0.1 eq.81
  37.4 0.1 fusion.21
  37.5 0.1 reduce_sum.12
  37.6 0.1 copy.35
  37.8 1.6 %convolution_convert_fusion.1 = bf16[896,512]{1,0:T(8,128)(2,1)} fusion(bf16[320,512]{1,0:T(8,128)(2,1)S(1)} %fusion.18, s32[320]{0:T(512)S(1)} %get-tuple-element.8, s32[320]{0:T(512)S(1)} %get-tuple-element.7), kind=kOutput, calls=%fused_computation.9 | convolution fusion | flops 294920192 | bytes 1247744 | tf_op jit(solution)/shard_map/dot_general | solution.py:502
  39.4 52.8 %dispatch.1 = bf16[8,112,2048]{2,1,0:T(8,128)(2,1)} custom-call(bf16[8,112,512]{2,1,0:T(8,128)(2,1)} %bitcast.50, f32[1,2048]{1,0:T(1,128)} %bitcast.53), custom_call_target="tpu_custom_call" | custom-call | tf_op jit(solution)/shard_map/dispatch/pallas_call | solution.py:427
  92.2 0.0 copy-start.1
  92.2 0.0 copy-start.5
  92.2 7.2 %fusion.2 = f32[896,896]{1,0:T(8,128)S(1)} fusion(bf16[896,2048]{1,0:T(8,128)(2,1)} %bitcast.45, bf16[1,2048,896]{2,1,0:T(8,128)(2,1)} %param.24), kind=kOutput, calls=%fused_computation.2 | convolution fusion | flops 3288334336 | bytes 10551296 | tf_op jit(solution)/shard_map/dot_general | solution.py:508
  99.4 0.0 copy-done.1
  99.4 0.0 copy-done.5
  99.5 0.0 copy-start.6
  99.5 4.2 %multiply_convert_fusion = bf16[896,896]{1,0:T(8,128)(2,1)S(1)} fusion(f32[896,896]{1,0:T(8,128)S(1)} %fusion.2, bf16[896,2048]{1,0:T(8,128)(2,1)S(1)} %bitcast.46, bf16[1,2048,896]{2,1,0:T(8,128)(2,1)S(1)} %copy-done.5), kind=kOutput, calls=%fused_computation.7 | convolution fusion | flops 3293151232 | bytes 12156928 | tf_op jit(solution)/shard_map/dot_general | solution.py:507
  103.7 0.0 copy-done.6
  103.7 5.4 %fusion.6 = bf16[896,2048]{1,0:T(8,128)(2,1)} fusion(bf16[896,896]{1,0:T(8,128)(2,1)S(1)} %multiply_convert_fusion, bf16[1,896,2048]{2,1,0:T(8,128)(2,1)S(1)} %copy-done.6), kind=kOutput, calls=%fused_computation.6 | convolution fusion | flops 3290169344 | bytes 8945664 | tf_op jit(solution)/shard_map/dot_general | solution.py:510
  109.1 0.0 copy-start.4
  109.1 33.0 %combine.1 = bf16[8,112,512]{2,1,0:T(8,128)(2,1)} custom-call(bf16[8,112,2048]{2,1,0:T(8,128)(2,1)} %bitcast.47), custom_call_target="tpu_custom_call" | custom-call | tf_op jit(solution)/shard_map/combine/pallas_call | solution.py:447
  142.1 0.0 copy-done.4
  142.1 1.7 %fusion.14 = f32[320,512]{1,0:T(8,128)S(1)} fusion(bf16[896,512]{1,0:T(8,128)(2,1)} %bitcast.48, bf16[320,512]{1,0:T(8,128)(2,1)S(1)} %fusion.18, s32[320]{0:T(512)S(1)} %get-tuple-element.7, f32[320]{0:T(512)S(1)} %get-tuple-element.6), kind=kOutput, calls=%fused_computation.16 | convolution fusion | flops 294379520 | bytes 1903104 | tf_op jit(solution)/shard_map/dot_general | solution.py:517
  143.8 2.5 %fusion.15 = bf16[320,512]{1,0:T(8,128)(2,1)} fusion(f32[320,512]{1,0:T(8,128)S(1)} %fusion.14, bf16[896,512]{1,0:T(8,128)(2,1)} %bitcast.49, s32[320]{0:T(512)S(1)} %get-tuple-element.8, f32[320]{0:T(512)S(1)} %get-tuple-element.5), kind=kOutput, calls=%fused_computation.17 | convolution fusion | flops 294379520 | bytes 1903104 | tf_op jit(solution)/shard_map/dot_general | solution.py:517
  (6 shorter events, 0.1 us)
Async XLA Ops:
  0.0 17.9 %copy-start = (bf16[256,2048]{1,0:T(8,128)(2,1)S(1)}, bf16[256,2048]{1,0:T(8,128)(2,1)}, u32[]{:S(2)}) copy-start(bf16[256,2048]{1,0:T(8,128)(2,1)} %param.18) | copy-start | bytes 3145732
  2.0 32.0 %copy-start.2 = (bf16[320,512]{1,0:T(8,128)(2,1)S(1)}, bf16[320,512]{1,0:T(8,128)(2,1)}, u32[]{:S(2)}) copy-start(bf16[320,512]{1,0:T(8,128)(2,1)} %param.19) | copy-start | bytes 983044
  2.8 32.3 %copy-start.3 = (s32[320,2]{0,1:T(2,128)S(1)}, s32[320,2]{0,1:T(2,128)}, u32[]{:S(2)}) copy-start(s32[320,2]{0,1:T(2,128)} %param.21) | copy-start | bytes 7684
  92.2 7.3 %copy-start.1 = (bf16[8,112,2048]{2,1,0:T(8,128)(2,1)S(1)}, bf16[8,112,2048]{2,1,0:T(8,128)(2,1)}, u32[]{:S(2)}) copy-start(bf16[8,112,2048]{2,1,0:T(8,128)(2,1)} %dispatch.1) | copy-start | bytes 11010052
  92.2 7.3 %copy-start.5 = (bf16[1,2048,896]{2,1,0:T(8,128)(2,1)S(1)}, bf16[1,2048,896]{2,1,0:T(8,128)(2,1)}, u32[]{:S(2)}) copy-start(bf16[1,2048,896]{2,1,0:T(8,128)(2,1)} %param.23) | copy-start | bytes 11010052
  99.5 4.2 %copy-start.6 = (bf16[1,896,2048]{2,1,0:T(8,128)(2,1)S(1)}, bf16[1,896,2048]{2,1,0:T(8,128)(2,1)}, u32[]{:S(2)}) copy-start(bf16[1,896,2048]{2,1,0:T(8,128)(2,1)} %param.25) | copy-start | bytes 11010052
  109.1 33.0 %copy-start.4 = (f32[320,2]{0,1:T(2,128)S(1)}, f32[320,2]{0,1:T(2,128)}, u32[]{:S(2)}) copy-start(f32[320,2]{0,1:T(2,128)} %param.22) | copy-start | bytes 7684
